TPU v7x, 32 devices: a whole 2x2x4 slice. The times are simulated.
32 devices in a mesh: grp: 2 (over y), sp: 4 (over z), tp: 4 (over x, core).
Axes of the slice: x: 2, y: 2, z: 4, core: 2. Of those that a mesh axis runs over, the one named last changes fastest.
Arguments:
- residual_in: bfloat16 [2048, 2048], P(('grp', 'sp', 'tp')), parts along dimension 0, may hold values from -6 to 6
- query_rows: bfloat16 [2048, 2048], P(('grp', 'sp'), 'tp'), parts along dimension 0, may hold values from -6 to 6
- key_rows: bfloat16 [2048, 512], P(('grp', 'sp'), 'tp'), parts along dimension 0, may hold values from -6 to 6
- value_rows: bfloat16 [2048, 512], P(('grp', 'sp'), 'tp'), parts along dimension 0, may hold values from -6 to 6
- forget_cumsum: float32 [2048, 16], P(('grp', 'sp'), 'tp'), parts along dimension 0, as said below
- head_gain: float32 [2048], P('tp'), may hold values from 0.1 to 1.9
- w_out: bfloat16 [2048, 2048], P('tp'), may hold values from -0.125 to 0.125
- w_up: bfloat16 [2048, 8192], P('sp', 'tp'), may hold values from -0.125 to 0.125
- w_down: bfloat16 [8192, 2048], P('tp', 'sp'), may hold values from -0.0625 to 0.0625
- mixer_gain: float32 [2048], replicated, may hold values from 0.1 to 1.9
- channel_gain: float32 [2048], replicated, may hold values from 0.1 to 1.9
Outputs:
- layer_out: bfloat16 [2048, 2048], P(('grp', 'sp', 'tp')), parts along dimension 0
There are 2 independent parts, one for each index of `grp`. A program takes and returns all parts, laid end to end along the dimension named above; an argument that names none is the same for every part. Nothing has to cross between parts.
Inputs may be any that keep to these rules, and one draw needn't show every extreme that they name: `forget_cumsum`: Non-positive; along the positions, each head's entries never rise.
All inputs are finite; a program needn't handle non-finite values.
Results may differ from a plain program's by a relative error of at most 0.015.
Values may be sent and summed in bfloat16 or wider, within the bound.
A program may use at most 128 MiB of HBM per device.

v0:
```python
import jax
import jax.numpy as jnp
from jax import lax
from jax.sharding import PartitionSpec as P

HD = 128
ALPHA = 8.0**0.25
EPSILON = 1e-05
NEG_FILL = -1e30


def layer_scale(inputs, gain_vec):
    centered = inputs - jnp.mean(inputs, axis=-1, keepdims=True)
    variance = jnp.mean(centered * centered, axis=-1, keepdims=True)
    return centered * lax.rsqrt(variance + EPSILON) * gain_vec


def shards(
    residual_in,
    query_rows,
    key_rows,
    value_rows,
    forget_cumsum,
    head_gain,
    w_out,
    w_up,
    w_down,
    mixer_gain,
    channel_gain,
):
    tok_rows = query_rows.shape[0]
    heads_here = forget_cumsum.shape[1]
    kv_here = key_rows.shape[1] // HD
    group_size = heads_here // kv_here
    score_scale = HD ** (-0.5)
    seq_index = lax.axis_index("sp")
    gate_all = lax.all_gather(forget_cumsum, "sp", axis=0, tiled=True)
    query_grid = query_rows.reshape(tok_rows, kv_here, group_size, HD)
    query_pos = seq_index * tok_rows + jnp.arange(tok_rows, dtype=jnp.int32)
    last_query = seq_index * tok_rows + tok_rows - 1
    gate_query = forget_cumsum.reshape(tok_rows, kv_here, group_size).transpose(1, 2, 0)

    def attend(carry_state, key_block, value_block, first_row):
        row_count = key_block.shape[0]

        def attend_live(live_state):
            peak_score, denom_sum, accum = live_state
            key_grid = key_block.reshape(row_count, kv_here, HD)
            value_grid = value_block.reshape(row_count, kv_here, HD)
            gate_block = lax.dynamic_slice_in_dim(gate_all, first_row, row_count, 0)
            gate_block = gate_block.reshape(row_count, kv_here, group_size).transpose(1, 2, 0)
            scores = (
                jnp.einsum(
                    "tkgd,ukd->kgtu", query_grid, key_grid, preferred_element_type=jnp.float32
                )
                * score_scale
            )
            scores = scores + gate_query[..., None] - gate_block[:, :, None, :]
            key_pos = first_row + jnp.arange(row_count, dtype=jnp.int32)
            allowed = key_pos[None, :] <= query_pos[:, None]
            scores = jnp.where(allowed, scores, NEG_FILL)
            new_peak = jnp.maximum(peak_score, jnp.max(scores, axis=-1))
            weights = jnp.where(allowed, jnp.exp(scores - new_peak[..., None]), 0.0)
            fade_factor = jnp.exp(peak_score - new_peak)
            denom_sum = denom_sum * fade_factor + jnp.sum(weights, axis=-1)
            accum = accum * fade_factor[..., None] + jnp.einsum(
                "kgtu,ukd->kgtd",
                weights.astype(jnp.bfloat16),
                value_grid,
                preferred_element_type=jnp.float32,
            )
            return (new_peak, denom_sum, accum)

        return lax.cond(
            first_row <= last_query, attend_live, lambda kept_state: kept_state, carry_state
        )

    def fold_keys(carry_state, pieces, first_row):
        key_piece, value_piece = pieces
        row_count = key_piece.shape[0]
        block_span = 1024
        if row_count > block_span and row_count % block_span == 0:

            def scan_block(scan_state, block_index):
                offset = block_index * block_span
                next_state = attend(
                    scan_state,
                    lax.dynamic_slice_in_dim(key_piece, offset, block_span, 0),
                    lax.dynamic_slice_in_dim(value_piece, offset, block_span, 0),
                    first_row + offset,
                )
                return (next_state, None)

            carry_state, unused = lax.scan(
                scan_block, carry_state, jnp.arange(row_count // block_span, dtype=jnp.int32)
            )
            return carry_state
        return attend(carry_state, key_piece, value_piece, first_row)

    fold_init = (
        jnp.full((kv_here, group_size, tok_rows), NEG_FILL, jnp.float32),
        jnp.zeros((kv_here, group_size, tok_rows), jnp.float32),
        jnp.zeros((kv_here, group_size, tok_rows, HD), jnp.float32),
    )
    peak_score, denom_sum, accum = fold_keys(
        fold_init,
        (
            lax.all_gather(key_rows, "sp", axis=0, tiled=True),
            lax.all_gather(value_rows, "sp", axis=0, tiled=True),
        ),
        jnp.int32(0),
    )
    attended = accum / denom_sum[..., None]
    normed = attended * lax.rsqrt(jnp.mean(attended * attended, axis=-1, keepdims=True) + EPSILON)
    normed = normed * head_gain.reshape(kv_here, group_size, 1, HD)
    heads_out = normed.transpose(2, 0, 1, 3).reshape(tok_rows, heads_here * HD).astype(jnp.bfloat16)
    branch = lax.psum_scatter(
        jnp.dot(heads_out, w_out, preferred_element_type=jnp.float32).astype(jnp.bfloat16),
        "tp",
        scatter_dimension=0,
        tiled=True,
    ).astype(jnp.float32)
    mid_rows = layer_scale(ALPHA * residual_in.astype(jnp.float32) + branch, mixer_gain).astype(
        jnp.bfloat16
    )
    mid_all = lax.all_gather(mid_rows, "tp", axis=0, tiled=True)
    up_full, down_full = (
        lax.all_gather(w_up, "sp", axis=0, tiled=True),
        lax.all_gather(w_down, "sp", axis=1, tiled=True),
    )
    lifted = jnp.dot(mid_all, up_full, preferred_element_type=jnp.float32)
    active = jnp.square(jax.nn.relu(lifted)).astype(jnp.bfloat16)
    lowered = lax.psum_scatter(
        jnp.dot(active, down_full, preferred_element_type=jnp.float32).astype(jnp.bfloat16),
        "tp",
        scatter_dimension=0,
        tiled=True,
    ).astype(jnp.float32)
    return layer_scale(ALPHA * mid_rows.astype(jnp.float32) + lowered, channel_gain).astype(
        jnp.bfloat16
    )


def solution(mesh):
    placed = (
        P(("grp", "sp", "tp"), None),
        P(("grp", "sp"), "tp"),
        P(("grp", "sp"), "tp"),
        P(("grp", "sp"), "tp"),
        P(("grp", "sp"), "tp"),
        P("tp"),
        P("tp", None),
        P("sp", "tp"),
        P("tp", "sp"),
        P(),
        P(),
    )
    return jax.shard_map(
        shards, mesh=mesh, in_specs=placed, out_specs=P(("grp", "sp", "tp"), None), check_vma=False
    )
```

profile of v0, /device:TPU:0, one launch (start us, length us, event | category | flops | bytes accessed | tf_op | source)
XLA Modules:
  0.0 451.6 jit_solution(16163317256759813407)
XLA Ops:
  6.5 16.0 %all_gather.18 = bf16[1024,128]{1,0:T(8,128)(2,1)S(1)} all-gather(bf16[256,128]{1,0:T(8,128)(2,1)} %param.15), channel_id=1, replica_groups=mesh['grp'=2,'sp'=4,'tp'=4] {'sp'}, dimensions={0}, use_global_device_ids=true | all-gather | bytes 327680 | tf_op jit(solution)/shard_map/all_gather | solution.py:108
  22.5 14.8 %all_gather.20 = bf16[1024,128]{1,0:T(8,128)(2,1)S(1)} all-gather(bf16[256,128]{1,0:T(8,128)(2,1)} %param.16), channel_id=1, replica_groups=mesh['grp'=2,'sp'=4,'tp'=4] {'sp'}, dimensions={0}, use_global_device_ids=true | all-gather | bytes 327680 | tf_op jit(solution)/shard_map/all_gather | solution.py:109
  37.4 13.3 %all_gather.19 = f32[1024,4]{0,1:T(4,128)S(1)} all-gather(f32[256,4]{0,1:T(4,128)} %param.17), channel_id=1, replica_groups=mesh['grp'=2,'sp'=4,'tp'=4] {'sp'}, dimensions={0}, use_global_device_ids=true | all-gather | bytes 20480 | tf_op jit(solution)/shard_map/all_gather | solution.py:37
  50.7 6.1 %conditional.1 = (f32[1,4,256]{2,1,0:T(4,128)S(1)}, f32[1,4,256,128]{2,3,1,0:T(8,128)S(1)}) conditional(s32[]{:T(128)} %convert_element_type.43, () %tuple.13, (s32[]{:T(128)}, s32[256]{0:T(256)S(1)}, bf16[256,512]{1,0:T(8,128)(2,1)}, bf16[1024,128]{1,0:T(8,128)(2,1)S(1)}, f32[1,4,256]{2,1,0:T(4,128)}, /*index=5*/f32[1024,4]{0,1:T(4,128)S(1)}, ...), branch_computations={%region_0.0_spmd, %region_1.4_spmd} | conditional | flops 557190400 | bytes 16116784 | solution.py:74
  50.7 0.2 iota_compare_fusion
  50.9 2.1 fusion.4
  53.0 1.5 fusion.3
  54.5 2.1 fusion.12
  56.6 0.2 copy.20
  56.8 0.1 multiply_reduce_fusion.2
  56.9 0.1 multiply_convert_fusion.2
  57.1 1.7 convolution_convert_fusion
  58.8 0.0 reduce-scatter.3.cloned.1.call-update
  58.8 0.0 all-gather.4.cloned.1.call-start
  58.9 25.8 %reduce-scatter.3.cloned.1.call-done = bf16[64,2048]{1,0:T(8,128)(2,1)} async-done(((bf16[256,2048]{1,0:T(8,128)(2,1)}), bf16[64,2048]{1,0:T(8,128)(2,1)}) %reduce-scatter.3.cloned.1.call-update) | async-done | bytes 262160 | tf_op jit(solution)/shard_map/reduce_scatter | solution.py:117
  84.7 1.1 fusion.25
  85.9 1.2 multiply_reduce_fusion.1
  87.1 1.8 multiply_convert_fusion.1
  88.9 0.0 all-gather.4.cloned.1.call-update
  88.9 0.0 all-gather.6.cloned.1.call-start
  88.9 0.7 all-gather.6.cloned.1.call-update
  89.6 0.0 all-gather.8.cloned.1.call-start
  89.7 0.5 all-gather.8.cloned.1.call-update
  90.2 0.0 reduce-scatter.5.cloned.1.call-start
  90.3 15.5 %all-gather.4.cloned.1.call-done = bf16[256,2048]{1,0:T(8,128)(2,1)} async-done(((bf16[64,2048]{1,0:T(8,128)(2,1)}), bf16[256,2048]{1,0:T(8,128)(2,1)}) %all-gather.4.cloned.1.call-update) | async-done | bytes 1048592 | tf_op jit(solution)/shard_map/all_gather | solution.py:126
  105.7 151.2 %all-gather.6.cloned.1.call-done = bf16[2048,2048]{1,0:T(8,128)(2,1)} async-done(((bf16[512,2048]{1,0:T(8,128)(2,1)}), bf16[2048,2048]{1,0:T(8,128)(2,1)}) %all-gather.6.cloned.1.call-update) | async-done | bytes 8388624 | tf_op jit(solution)/shard_map/all_gather | solution.py:128
  257.0 149.3 %all-gather.8.cloned.1.call-done = bf16[2048,2048]{1,0:T(8,128)(2,1)} async-done(((bf16[2048,512]{1,0:T(8,128)(2,1)}), bf16[2048,2048]{1,0:T(8,128)(2,1)}) %all-gather.8.cloned.1.call-update) | async-done | bytes 8388624 | tf_op jit(solution)/shard_map/all_gather | solution.py:129
  406.2 11.6 %convolution_convert_fusion.1 = bf16[256,2048]{1,0:T(8,128)(2,1)} fusion(bf16[2048,2048]{1,0:T(8,128)(2,1)} %all-gather.8.cloned.1.call-done, bf16[256,2048]{1,0:T(8,128)(2,1)} %all-gather.4.cloned.1.call-done, bf16[2048,2048]{1,0:T(8,128)(2,1)} %all-gather.6.cloned.1.call-done), kind=kOutput, calls=%fused_computation.29 | convolution fusion | flops 4297064448 | bytes 18874368 | tf_op jit(solution)/shard_map/dot_general | solution.py:134
  417.8 23.1 %reduce-scatter.5.cloned.1.call-done = bf16[64,2048]{1,0:T(8,128)(2,1)} async-done(((bf16[256,2048]{1,0:T(8,128)(2,1)}), bf16[64,2048]{1,0:T(8,128)(2,1)}) %reduce-scatter.5.cloned.1.call-update) | async-done | bytes 262160 | tf_op jit(solution)/shard_map/reduce_scatter | solution.py:133
  440.9 1.1 fusion.26
  442.0 1.2 multiply_reduce_fusion
  443.2 1.8 multiply_convert_fusion
  (25 shorter events, 0.1 us)
Async XLA Ops:
  6.5 50.5 %copy-start = (bf16[512,2048]{1,0:T(8,128)(2,1)S(1)}, bf16[512,2048]{1,0:T(8,128)(2,1)}, u32[]{:S(2)}) copy-start(bf16[512,2048]{1,0:T(8,128)(2,1)} %param.19) | copy-start | bytes 6291460
  6.5 78.2 %reduce-scatter.3.cloned.1.call-start = ((), (), s32[]{:S(2)}) async-start(), calls=%async_computation.2 | async-start | bytes 1310720 | tf_op jit(solution)/shard_map/reduce_scatter | solution.py:117
  50.7 6.2 %copy-start.6 = (f32[512]{0:T(512)S(1)}, f32[512]{0:T(512)}, u32[]{:S(2)}) copy-start(f32[512]{0:T(512)} %param.18) | copy-start | bytes 6148
  50.7 2.3 copy-start.3
  56.8 27.9 %copy-start.2 = (bf16[64,2048]{1,0:T(8,128)(2,1)S(1)}, bf16[64,2048]{1,0:T(8,128)(2,1)}, u32[]{:S(2)}) copy-start(bf16[64,2048]{1,0:T(8,128)(2,1)} %param.13) | copy-start | bytes 786436
  56.8 30.2 %copy-start.4 = (f32[2048]{0:T(1024)S(1)}, f32[2048]{0:T(1024)}, u32[]{:S(2)}) copy-start(f32[2048]{0:T(1024)} %param.22) | copy-start | bytes 24580
  58.8 46.9 %all-gather.4.cloned.1.call-start = ((), (), s32[]{:S(2)}) async-start(), calls=%async_computation.3 | async-start | bytes 1310720 | tf_op jit(solution)/shard_map/all_gather | solution.py:126
  88.9 168.1 %all-gather.6.cloned.1.call-start = ((), (), s32[]{:S(2)}) async-start(), calls=%async_computation.4 | async-start | bytes 10485760 | tf_op jit(solution)/shard_map/all_gather | solution.py:128
  89.6 316.6 %all-gather.8.cloned.1.call-start = ((), (), s32[]{:S(2)}) async-start(), calls=%async_computation.5 | async-start | bytes 10485760 | tf_op jit(solution)/shard_map/all_gather | solution.py:129
  90.2 350.7 %copy-start.1 = (bf16[64,2048]{1,0:T(8,128)(2,1)S(1)}, bf16[64,2048]{1,0:T(8,128)(2,1)}, u32[]{:S(2)}) copy-start(bf16[64,2048]{1,0:T(8,128)(2,1)} %multiply_convert_fusion.1) | copy-start | bytes 786436
  90.2 353.0 %copy-start.5 = (f32[2048]{0:T(1024)S(1)}, f32[2048]{0:T(1024)}, u32[]{:S(2)}) copy-start(f32[2048]{0:T(1024)} %param.23) | copy-start | bytes 24580
  90.2 350.7 %reduce-scatter.5.cloned.1.call-start = ((), (), s32[]{:S(2)}) async-start(), calls=%async_computation.6 | async-start | bytes 1310720 | tf_op jit(solution)/shard_map/reduce_scatter | solution.py:133
Sparse Core Ops, SparseCore 0:
  59.0 25.7 reduce-scatter.2
  89.0 16.6 all-gather.3
  107.3 149.6 all-gather.5
  258.4 147.7 all-gather.7
  417.9 22.9 reduce-scatter.4
where the time goes:
time: 452 us
  waiting for transfers between devices  366 us (81%)
  blocking collectives  44.2 us (10%)
  matrix products  17.5 us (4%)
  between operations  13.3 us (3%)
  other arithmetic  10.1 us (2%)
    all_gather x1, waiting for transfers between devices, shards(): lax.all_gather(w_up, 'sp', axis=0, tiled=True)  151 us
    all_gather x1, waiting for transfers between devices, shards(): lax.all_gather(w_down, 'sp', axis=1, tiled=True)  149 us
    reduce_scatter x1, waiting for transfers between devices, shards(): lax.psum_scatter(jnp.dot(heads_out, w_out, preferred_element_type=jnp.flo...  25.8 us
    reduce_scatter x1, waiting for transfers between devices, shards(): lax.psum_scatter(jnp.dot(active, down_full, preferred_element_type=jnp.fl...  23.1 us
    all_gather x1, blocking collectives, shards(): lax.all_gather(key_rows, 'sp', axis=0, tiled=True)  16 us
    all_gather x1, waiting for transfers between devices, shards(): mid_all = lax.all_gather(mid_rows, 'tp', axis=0, tiled=True)  15.5 us
    all_gather x1, blocking collectives, shards(): lax.all_gather(value_rows, 'sp', axis=0, tiled=True)  14.8 us
    all_gather x1, blocking collectives, shards(): gate_all = lax.all_gather(forget_cumsum, 'sp', axis=0, tiled=True)  13.3 us
  transfers between devices with their start and end apart: 5, of which 5 were waited for; matrix products, arithmetic and copies ran while one was open for 0% of the time, Pallas kernels for 0%

commit v1 on v0

--- a/solution.py
+++ b/solution.py
@@ -7,6 +7,11 @@
 ALPHA = 8.0**0.25
 EPSILON = 1e-05
 NEG_FILL = -1e30
+
+
+def all_parts(block, name, d):
+    blocks = lax.all_gather(block, name)
+    return jnp.concatenate(blocks, axis=d)
 
 
 def layer_scale(inputs, gain_vec):
@@ -126,7 +131,7 @@
     mid_all = lax.all_gather(mid_rows, "tp", axis=0, tiled=True)
     up_full, down_full = (
         lax.all_gather(w_up, "sp", axis=0, tiled=True),
-        lax.all_gather(w_down, "sp", axis=1, tiled=True),
+        all_parts(w_down, "sp", 1),
     )
     lifted = jnp.dot(mid_all, up_full, preferred_element_type=jnp.float32)
     active = jnp.square(jax.nn.relu(lifted)).astype(jnp.bfloat16)

time: 452 us -> 427 us (0.945)
  waiting for transfers between devices: 366 us -> 326 us
  local copies, waits for them, and re-layouts: 0.24 us -> 11.7 us
    all_gather x1, waiting for transfers between devices: 149 us -> 122 us  [all_parts(): blocks = lax.all_gather(block, name)]
    reshape x0 -> x1, local copies, waits for them, and re-layouts: none -> 11.5 us  [all_parts(): return jnp.concatenate(blocks, axis=d)]
    all_gather x1, waiting for transfers between devices: 15.5 us -> 4.73 us  [shards(): mid_all = lax.all_gather(mid_rows, 'tp', axis=0, tiled=True)]
  transfers between devices with their start and end apart: 5 -> 5, of which waited for: 5 -> 5; matrix products, arithmetic and copies ran while one was open for 0% -> 4% of each run, Pallas kernels for 0% -> 0%
where the time goes in v1:
time: 427 us
  waiting for transfers between devices  326 us (76%)
  blocking collectives  45.7 us (11%)
  matrix products  17.6 us (4%)
  between operations  15.1 us (4%)
  local copies, waits for them, and re-layouts  11.7 us (3%)
  other arithmetic  10.1 us (2%)
    all_gather x1, waiting for transfers between devices, shards(): lax.all_gather(w_up, 'sp', axis=0, tiled=True)  151 us
    all_gather x1, waiting for transfers between devices, all_parts(): blocks = lax.all_gather(block, name)  122 us
    reduce_scatter x1, waiting for transfers between devices, shards(): lax.psum_scatter(jnp.dot(heads_out, w_out, preferred_element_type=jnp.flo...  24.4 us
    reduce_scatter x1, waiting for transfers between devices, shards(): lax.psum_scatter(jnp.dot(active, down_full, preferred_element_type=jnp.fl...  23.1 us
    all_gather x1, blocking collectives, shards(): lax.all_gather(value_rows, 'sp', axis=0, tiled=True)  16.4 us
    all_gather x1, blocking collectives, shards(): lax.all_gather(key_rows, 'sp', axis=0, tiled=True)  16 us
    all_gather x1, blocking collectives, shards(): gate_all = lax.all_gather(forget_cumsum, 'sp', axis=0, tiled=True)  13.3 us
    dot_general x1, matrix products, shards(): jnp.dot(active, down_full, preferred_element_type=jnp.float32)  11.6 us
  transfers between devices with their start and end apart: 5, of which 5 were waited for; matrix products, arithmetic and copies ran while one was open for 4% of the time, Pallas kernels for 0%

profile of v1, /device:TPU:0, one launch (start us, length us, event | category | flops | bytes accessed | tf_op | source)
XLA Modules:
  0.0 426.6 jit_solution(2649168089818737585)
XLA Ops:
  7.4 16.0 %all_gather.21 = bf16[1024,128]{1,0:T(8,128)(2,1)S(1)} all-gather(bf16[256,128]{1,0:T(8,128)(2,1)} %param.15), channel_id=1, replica_groups=mesh['grp'=2,'sp'=4,'tp'=4] {'sp'}, dimensions={0}, use_global_device_ids=true | all-gather | bytes 327680 | tf_op jit(solution)/shard_map/all_gather | solution.py:113
  23.4 16.4 %all_gather.23 = bf16[1024,128]{1,0:T(8,128)(2,1)} all-gather(bf16[256,128]{1,0:T(8,128)(2,1)} %param.16), channel_id=1, replica_groups=mesh['grp'=2,'sp'=4,'tp'=4] {'sp'}, dimensions={0}, use_global_device_ids=true | all-gather | bytes 327680 | tf_op jit(solution)/shard_map/all_gather | solution.py:114
  39.7 13.3 %all_gather.22 = f32[1024,4]{0,1:T(4,128)S(1)} all-gather(f32[256,4]{0,1:T(4,128)} %param.17), channel_id=1, replica_groups=mesh['grp'=2,'sp'=4,'tp'=4] {'sp'}, dimensions={0}, use_global_device_ids=true | all-gather | bytes 20480 | tf_op jit(solution)/shard_map/all_gather | solution.py:42
  53.1 6.1 %conditional.1 = (f32[1,4,256]{2,1,0:T(4,128)S(1)}, f32[1,4,256,128]{2,3,1,0:T(8,128)S(1)}) conditional(s32[]{:T(128)} %convert_element_type.43, () %tuple.13, (s32[]{:T(128)}, s32[256]{0:T(256)S(1)}, bf16[256,512]{1,0:T(8,128)(2,1)}, bf16[1024,128]{1,0:T(8,128)(2,1)S(1)}, f32[1,4,256]{2,1,0:T(4,128)}, /*index=5*/f32[1024,4]{0,1:T(4,128)S(1)}, ...), branch_computations={%region_0.0_spmd, %region_1.4_spmd} | conditional | flops 557190400 | bytes 17165388 | solution.py:79
  53.1 0.2 iota_compare_fusion
  53.3 2.1 fusion.4
  55.4 1.5 fusion.3
  57.0 2.0 fusion.12
  59.0 0.2 copy.24
  59.2 0.1 multiply_reduce_fusion.2
  59.3 0.1 multiply_convert_fusion.2
  59.5 1.8 convolution_convert_fusion
  61.3 0.0 all-gather.9.cloned.1.call-start
  61.4 0.5 all-gather.9.cloned.1.call-update
  61.9 0.0 all-gather.5.cloned.1.call-start
  61.9 24.4 %reduce-scatter.3.cloned.1.call-done = bf16[64,2048]{1,0:T(8,128)(2,1)} async-done(((bf16[256,2048]{1,0:T(8,128)(2,1)}), bf16[64,2048]{1,0:T(8,128)(2,1)}) %reduce-scatter.3.cloned.1.call-update) | async-done | bytes 262160 | tf_op jit(solution)/shard_map/reduce_scatter | solution.py:122
  86.3 1.1 fusion.25
  87.5 1.2 multiply_reduce_fusion.1
  88.7 1.8 multiply_convert_fusion.1
  90.5 0.0 all-gather.5.cloned.1.call-update
  90.5 0.0 all-gather.7.cloned.1.call-start
  90.5 0.5 all-gather.7.cloned.1.call-update
  91.1 0.0 reduce-scatter.5.cloned.1.call-start
  91.1 121.8 %all-gather.9.cloned.1.call-done = bf16[8192,512]{1,0:T(8,128)(2,1)} async-done(((bf16[2048,512]{1,0:T(8,128)(2,1)}), bf16[8192,512]{1,0:T(8,128)(2,1)}) %all-gather.9.cloned.1.call-update) | async-done | bytes 8388624 | tf_op jit(solution)/shard_map/all_gather | solution.py:13
  212.9 11.5 %copy.21 = bf16[2048,4,512]{0,2,1:T(8,128)(2,1)} copy(bf16[2048,4,512]{2,0,1:T(8,128)(2,1)} %bitcast.72) | data formatting | bytes 16777216 | tf_op jit(solution)/shard_map/reshape | solution.py:14
  224.4 4.7 %all-gather.5.cloned.1.call-done = bf16[256,2048]{1,0:T(8,128)(2,1)} async-done(((bf16[64,2048]{1,0:T(8,128)(2,1)}), bf16[256,2048]{1,0:T(8,128)(2,1)}) %all-gather.5.cloned.1.call-update) | async-done | bytes 1048592 | tf_op jit(solution)/shard_map/all_gather | solution.py:131
  229.1 150.9 %all-gather.7.cloned.1.call-done = bf16[2048,2048]{1,0:T(8,128)(2,1)} async-done(((bf16[512,2048]{1,0:T(8,128)(2,1)}), bf16[2048,2048]{1,0:T(8,128)(2,1)}) %all-gather.7.cloned.1.call-update) | async-done | bytes 8388624 | tf_op jit(solution)/shard_map/all_gather | solution.py:133
  380.1 11.6 %convolution_convert_fusion.1 = bf16[256,2048]{1,0:T(8,128)(2,1)} fusion(bf16[2048,2048]{0,1:T(8,128)(2,1)} %bitcast.73, bf16[256,2048]{1,0:T(8,128)(2,1)} %all-gather.5.cloned.1.call-done, bf16[2048,2048]{1,0:T(8,128)(2,1)} %all-gather.7.cloned.1.call-done), kind=kOutput, calls=%fused_computation.29 | convolution fusion | flops 4297064448 | bytes 18874368 | tf_op jit(solution)/shard_map/dot_general | solution.py:139
  391.7 23.1 %reduce-scatter.5.cloned.1.call-done = bf16[64,2048]{1,0:T(8,128)(2,1)} async-done(((bf16[256,2048]{1,0:T(8,128)(2,1)}), bf16[64,2048]{1,0:T(8,128)(2,1)}) %reduce-scatter.5.cloned.1.call-update) | async-done | bytes 262160 | tf_op jit(solution)/shard_map/reduce_scatter | solution.py:138
  414.8 1.1 fusion.26
  416.0 1.2 multiply_reduce_fusion
  417.2 1.8 multiply_convert_fusion
  (28 shorter events, 0.1 us)
Async XLA Ops:
  7.4 52.1 %copy-start = (bf16[512,2048]{1,0:T(8,128)(2,1)S(1)}, bf16[512,2048]{1,0:T(8,128)(2,1)}, u32[]{:S(2)}) copy-start(bf16[512,2048]{1,0:T(8,128)(2,1)} %param.19) | copy-start | bytes 6291460
  7.4 78.9 %reduce-scatter.3.cloned.1.call-start = ((), (), s32[]{:S(2)}) async-start(), calls=%async_computation.2 | async-start | bytes 1310720 | tf_op jit(solution)/shard_map/reduce_scatter | solution.py:122
  53.1 6.2 %copy-start.7 = (f32[512]{0:T(512)S(1)}, f32[512]{0:T(512)}, u32[]{:S(2)}) copy-start(f32[512]{0:T(512)} %param.18) | copy-start | bytes 6148
  53.1 2.4 copy-start.4
  53.3 3.7 copy-start.3
  59.2 27.1 %copy-start.2 = (bf16[64,2048]{1,0:T(8,128)(2,1)S(1)}, bf16[64,2048]{1,0:T(8,128)(2,1)}, u32[]{:S(2)}) copy-start(bf16[64,2048]{1,0:T(8,128)(2,1)} %param.13) | copy-start | bytes 786436
  59.3 29.3 %copy-start.5 = (f32[2048]{0:T(1024)S(1)}, f32[2048]{0:T(1024)}, u32[]{:S(2)}) copy-start(f32[2048]{0:T(1024)} %param.22) | copy-start | bytes 24580
  61.3 151.6 %all-gather.9.cloned.1.call-start = ((), (), s32[]{:S(2)}) async-start(), calls=%async_computation.6 | async-start | bytes 10485760 | tf_op jit(solution)/shard_map/all_gather | solution.py:13
  61.9 167.2 %all-gather.5.cloned.1.call-start = ((), (), s32[]{:S(2)}) async-start(), calls=%async_computation.3 | async-start | bytes 1310720 | tf_op jit(solution)/shard_map/all_gather | solution.py:131
  90.5 289.6 %all-gather.7.cloned.1.call-start = ((), (), s32[]{:S(2)}) async-start(), calls=%async_computation.4 | async-start | bytes 10485760 | tf_op jit(solution)/shard_map/all_gather | solution.py:133
  91.1 323.8 %reduce-scatter.5.cloned.1.call-start = ((), (), s32[]{:S(2)}) async-start(), calls=%async_computation.5 | async-start | bytes 1310720 | tf_op jit(solution)/shard_map/reduce_scatter | solution.py:138
  380.1 34.7 %copy-start.1 = (bf16[64,2048]{1,0:T(8,128)(2,1)S(1)}, bf16[64,2048]{1,0:T(8,128)(2,1)}, u32[]{:S(2)}) copy-start(bf16[64,2048]{1,0:T(8,128)(2,1)} %multiply_convert_fusion.1) | copy-start | bytes 786436
  380.1 37.1 %copy-start.6 = (f32[2048]{0:T(1024)S(1)}, f32[2048]{0:T(1024)}, u32[]{:S(2)}) copy-start(f32[2048]{0:T(1024)} %param.23) | copy-start | bytes 24580
Sparse Core Ops, SparseCore 0:
  61.4 24.8 reduce-scatter.2
  391.9 22.9 reduce-scatter.4
Sparse Core Ops, SparseCore 1:
  63.4 149.5 all-gather.8
  214.4 14.7 all-gather.4
  230.6 149.4 all-gather.6
